TPU v7x, 32 devices: a whole 2x2x4 slice. The times are simulated.
32 devices in a mesh: ep: 8 (over z, x), tp: 4 (over y, core).
Axes of the slice: x: 2, y: 2, z: 4, core: 2. Of those that a mesh axis runs over, the one named last changes fastest.
Arguments:
- query_rows: bfloat16 [2048, 1024], P('ep', 'tp'), may hold values from -8 to 8
- key_rows: bfloat16 [2048, 256], P('ep', 'tp'), may hold values from -8 to 8
- value_rows: bfloat16 [2048, 256], P('ep', 'tp'), may hold values from -16 to 16
- query_gain: float32 [64], replicated, may hold values from 0.5 to 7.5
- key_gain: float32 [64], replicated, may hold values from 0.5 to 7.5
- moe_tokens: bfloat16 [4096, 2048], P(('ep', 'tp')), may hold values from -6 to 6
- norm_gain: float32 [2048], replicated, may hold values from 0.1 to 1.9
- routes: int32 [4096, 2], P('ep'), may hold values from 0 to 7, all different within a row; in each aligned block of 128 rows (0 to 127, 128 to 255, ...) at most 64 rows name the same one
- route_weights: float32 [4096, 2], P('ep'), may hold values from 0.1 to 1
- expert_gate: bfloat16 [8, 2048, 1024], P('ep', None, 'tp'), may hold values from -0.125 to 0.125
- expert_up: bfloat16 [8, 2048, 1024], P('ep', None, 'tp'), may hold values from -0.125 to 0.125
- expert_down: bfloat16 [8, 1024, 2048], P('ep', 'tp'), may hold values from -0.1875 to 0.1875
- shared_gate: bfloat16 [2048, 1024], P(None, 'tp'), may hold values from -0.125 to 0.125
- shared_up: bfloat16 [2048, 1024], P(None, 'tp'), may hold values from -0.125 to 0.125
- shared_down: bfloat16 [1024, 2048], P('tp'), may hold values from -0.1875 to 0.1875
Outputs:
- attn_out: bfloat16 [2048, 1024], P('ep', 'tp')
- moe_out: bfloat16 [4096, 2048], P(('ep', 'tp'))
Inputs may be any that keep to these rules, and one draw needn't show every extreme that they name: `routes`: each row names 2 different experts. Within each aligned block of 128 rows no expert is named more than 64 times, and in every draw some expert is named exactly 64 times in some block.
All inputs are finite; a program needn't handle non-finite values.
Results may differ from a plain program's by a relative error of at most 0.012.
The roundings to bfloat16 on the way count: a program that leaves them out, or rounds other values in their place, can miss the bound.
Values may be sent and summed in bfloat16 or wider, within the bound.
A program may use at most 192 MiB of HBM per device.

v0:
```python
import jax
import jax.numpy as jnp
from jax import lax
from jax.sharding import PartitionSpec as P

GRID_W = 64


epsilon = 1e-06
rotary_base = 10000.0
routed_scale = 2.5


def rotate_heads(heads_in, gain_row, positions):
    values32 = heads_in.astype(jnp.float32)
    scaled = (
        values32
        * lax.rsqrt(jnp.mean(values32 * values32, axis=-1, keepdims=True) + epsilon)
        * gain_row
    )
    pair_count = scaled.shape[-1] // 4
    inv_freq = rotary_base ** (-jnp.arange(pair_count, dtype=jnp.float32) / pair_count)
    grid_row = (positions // GRID_W).astype(jnp.float32)
    grid_col = (positions % GRID_W).astype(jnp.float32)
    angles = jnp.concatenate([grid_row[:, None] * inv_freq, grid_col[:, None] * inv_freq], axis=-1)[
        :, None, :
    ]
    cosine = jnp.cos(angles)
    sine_part = jnp.sin(angles)
    first_half = scaled[..., 0::2]
    second_half = scaled[..., 1::2]
    turned = jnp.stack(
        [
            first_half * cosine - second_half * sine_part,
            first_half * sine_part + second_half * cosine,
        ],
        axis=-1,
    )
    return turned.reshape(scaled.shape).astype(jnp.bfloat16)


def span_length(row_count):
    length = min(row_count, 2048)
    while row_count % length:
        length -= 1
    return length


def attend(query_rows, key_rows, value_rows, query_gain, key_gain):
    row_count = query_rows.shape[0]
    head_size = query_gain.shape[0]
    q_heads = query_rows.shape[1] // head_size
    kv_heads = key_rows.shape[1] // head_size
    group = q_heads // kv_heads
    scale = head_size ** (-0.5)
    positions = lax.axis_index("ep") * row_count + jnp.arange(row_count, dtype=jnp.int32)
    q_rot = rotate_heads(query_rows.reshape(row_count, q_heads, head_size), query_gain, positions)
    k_rot = rotate_heads(key_rows.reshape(row_count, kv_heads, head_size), key_gain, positions)
    key_value = jnp.stack([k_rot, value_rows.reshape(row_count, kv_heads, head_size)], axis=2)
    key_value = key_value.reshape(row_count, kv_heads * 2 * head_size)
    q_grouped = q_rot.reshape(row_count, kv_heads, group, head_size).transpose(1, 2, 0, 3)
    q_grouped = q_grouped.reshape(kv_heads, group * row_count, head_size)
    query_count = group * row_count
    initial = (
        jnp.full((kv_heads, query_count), -jnp.inf, jnp.float32),
        jnp.zeros((kv_heads, query_count), jnp.float32),
        jnp.zeros((kv_heads, query_count, head_size), jnp.float32),
    )

    def one_span(carried, span_rows):
        run_max, run_sum, mixed = carried
        keys_span = span_rows[:, :, 0, :]
        values_span = span_rows[:, :, 1, :]
        scores = (
            jnp.einsum("hrd,shd->hrs", q_grouped, keys_span, preferred_element_type=jnp.float32)
            * scale
        )
        new_max = jnp.maximum(run_max, jnp.max(scores, axis=-1))
        factor = jnp.exp(run_max - new_max)
        weights = jnp.exp(scores - new_max[..., None])
        run_sum = run_sum * factor + jnp.sum(weights, axis=-1)
        added = jnp.einsum(
            "hrs,shd->hrd",
            weights.astype(jnp.bfloat16),
            values_span,
            preferred_element_type=jnp.float32,
        )
        mixed = mixed * factor[..., None] + added
        return ((new_max, run_sum, mixed), None)

    carried = initial
    piece_rows = lax.all_gather(key_value, "ep", axis=0, tiled=True)
    piece_count = piece_rows.shape[0]
    length = span_length(piece_count)
    spans = piece_rows.reshape(piece_count // length, length, kv_heads, 2, head_size)
    carried, unused = lax.scan(one_span, carried, spans)
    run_max, run_sum, mixed = carried
    result = (mixed / run_sum[..., None]).astype(jnp.bfloat16)
    result = result.reshape(kv_heads, group, row_count, head_size).transpose(2, 0, 1, 3)
    return result.reshape(row_count, q_heads * head_size)


def slot_ranks(route_rows, tok_rows, experts):
    top_count = route_rows.shape[1]
    blocks = route_rows.shape[0] // tok_rows
    chosen = route_rows.reshape(blocks, tok_rows * top_count)
    one_hot = (chosen[:, :, None] == jnp.arange(experts, dtype=jnp.int32)[None, None, :]).astype(
        jnp.int32
    )
    ranks = jnp.sum((jnp.cumsum(one_hot, axis=1) - one_hot) * one_hot, axis=2)
    return (chosen, ranks)


def build_send(source, chosen, ranks, tok_rows, top_count, capacity, experts):
    blocks = chosen.shape[0]
    model_width = source.shape[1]
    block_ids = jnp.arange(blocks, dtype=jnp.int32)[:, None]
    dest = (chosen * blocks + block_ids) * capacity + ranks
    rows_from = (
        block_ids * tok_rows
        + jnp.arange(tok_rows * top_count, dtype=jnp.int32)[None, :] // top_count
    )
    slot_rows = jnp.full((experts * blocks * capacity,), blocks * tok_rows, jnp.int32)
    slot_rows = slot_rows.at[dest.reshape(-1)].set(rows_from.reshape(-1))
    padded = jnp.concatenate([source, jnp.zeros((1, model_width), source.dtype)], axis=0)
    return padded[slot_rows].reshape(experts, blocks * capacity, model_width)


def expert_products(arrived, w_gate, w_up, w_down):
    gate_proj = jnp.einsum("lrd,ldf->lrf", arrived, w_gate, preferred_element_type=jnp.float32)
    up_proj = jnp.einsum("lrd,ldf->lrf", arrived, w_up, preferred_element_type=jnp.float32)
    hidden = (jax.nn.silu(gate_proj) * up_proj).astype(jnp.bfloat16)
    return jnp.einsum("lrf,lfd->lrd", hidden, w_down, preferred_element_type=jnp.float32)


def shared_products(rows_in, w_gate, w_up, w_down):
    gate_proj = jnp.dot(rows_in, w_gate, preferred_element_type=jnp.float32)
    up_proj = jnp.dot(rows_in, w_up, preferred_element_type=jnp.float32)
    hidden = (jax.nn.silu(gate_proj) * up_proj).astype(jnp.bfloat16)
    return jnp.dot(hidden, w_down, preferred_element_type=jnp.float32)


def experts_half(
    moe_tokens,
    norm_gain,
    routes,
    route_weights,
    expert_gate,
    expert_up,
    expert_down,
    shared_gate,
    shared_up,
    shared_down,
):
    tok_rows, model_width = moe_tokens.shape
    top_count = routes.shape[1]
    tp_size = lax.axis_size("tp")
    ep_size = lax.axis_size("ep")
    local_experts = expert_gate.shape[0]
    experts = local_experts * ep_size
    capacity = 2 * tok_rows * top_count // experts
    lane = lax.axis_index("tp")
    values32 = moe_tokens.astype(jnp.float32)
    normed = (
        values32
        * lax.rsqrt(jnp.mean(values32 * values32, axis=-1, keepdims=True) + epsilon)
        * norm_gain
    ).astype(jnp.bfloat16)
    gates = route_weights / jnp.sum(route_weights, axis=-1, keepdims=True) * routed_scale
    own_gates = lax.dynamic_slice_in_dim(gates, lane * tok_rows, tok_rows, 0)
    own_routes = lax.dynamic_slice_in_dim(routes, lane * tok_rows, tok_rows, 0)
    chosen, ranks = slot_ranks(own_routes, tok_rows, experts)
    send = build_send(normed, chosen, ranks, tok_rows, top_count, capacity, experts)
    landed = lax.all_to_all(send, "ep", split_axis=0, concat_axis=1, tiled=True)
    arrived, group_rows = (
        lax.all_gather(
            landed.reshape(local_experts, ep_size, 1, capacity, model_width),
            "tp",
            axis=2,
            tiled=True,
        ),
        lax.all_gather(normed.reshape(1, 1, 1, tok_rows, model_width), "tp", axis=2, tiled=True),
    )
    own_chosen = chosen[0]
    own_ranks = ranks[0]
    arrived = arrived.reshape(local_experts, ep_size * tp_size * capacity, model_width)
    routed_part = expert_products(arrived, expert_gate, expert_up, expert_down)
    shared_part = shared_products(
        group_rows.reshape(tp_size * tok_rows, model_width), shared_gate, shared_up, shared_down
    )
    routed_sum, shared_sum = (
        lax.psum_scatter(
            routed_part.reshape(local_experts, ep_size, tp_size, capacity, model_width).astype(
                jnp.bfloat16
            ),
            "tp",
            scatter_dimension=2,
            tiled=True,
        ).astype(jnp.float32),
        lax.psum_scatter(
            shared_part.reshape(1, 1, tp_size, tok_rows, model_width).astype(jnp.bfloat16),
            "tp",
            scatter_dimension=2,
            tiled=True,
        ).astype(jnp.float32),
    )
    outgoing = routed_sum.astype(jnp.bfloat16).reshape(
        local_experts, ep_size * capacity, model_width
    )
    returned = lax.all_to_all(outgoing, "ep", split_axis=1, concat_axis=0, tiled=True)
    flat_rows = returned.reshape(experts * capacity, model_width)
    picked = flat_rows[own_chosen * capacity + own_ranks].reshape(tok_rows, top_count, model_width)
    routed_total = jnp.sum(own_gates[:, :, None] * picked.astype(jnp.float32), axis=1)
    return (routed_total + shared_sum.reshape(tok_rows, model_width)).astype(jnp.bfloat16)


def body(
    query_rows,
    key_rows,
    value_rows,
    query_gain,
    key_gain,
    moe_tokens,
    norm_gain,
    routes,
    route_weights,
    expert_gate,
    expert_up,
    expert_down,
    shared_gate,
    shared_up,
    shared_down,
):
    attn_out = attend(query_rows, key_rows, value_rows, query_gain, key_gain)
    moe_out = experts_half(
        moe_tokens,
        norm_gain,
        routes,
        route_weights,
        expert_gate,
        expert_up,
        expert_down,
        shared_gate,
        shared_up,
        shared_down,
    )
    return (attn_out, moe_out)


def solution(mesh):
    return jax.shard_map(
        body,
        mesh=mesh,
        in_specs=(
            P("ep", "tp"),
            P("ep", "tp"),
            P("ep", "tp"),
            P(),
            P(),
            P(("ep", "tp"), None),
            P(),
            P("ep", None),
            P("ep", None),
            P("ep", None, "tp"),
            P("ep", None, "tp"),
            P("ep", "tp", None),
            P(None, "tp"),
            P(None, "tp"),
            P("tp", None),
        ),
        out_specs=(P("ep", "tp"), P(("ep", "tp"), None)),
        check_vma=False,
    )
```

profile of v0, /device:TPU:0, one launch (start us, length us, event | category | flops | bytes accessed | tf_op | source)
XLA Modules:
  0.0 441.3 jit_solution(13202950709804458420)
XLA Ops:
  7.2 0.0 copy-start
  7.2 0.0 all-gather.5.cloned.1.call-start
  7.2 0.8 broadcast_multiply_fusion.2
  8.0 0.1 copy.45
  8.1 0.1 eq.30
  8.3 0.6 reduce-window.6
  8.9 0.2 slice_reduce_fusion
  9.1 0.1 fusion.44
  9.2 0.1 copy.44
  9.3 0.1 mul.289
  9.5 1.4 scatter_custom_fusion
  10.9 1.2 fusion.15
  12.2 1.2 fusion.17
  13.4 0.0 copy-start.2
  13.5 3.3 gather_fusion
  16.8 55.6 %all_to_all.8 = bf16[8,64,2048]{2,1,0:T(8,128)(2,1)} all-to-all(bf16[8,64,2048]{2,1,0:T(8,128)(2,1)} %bitcast.110), channel_id=1, replica_groups=mesh['ep'=8,'tp'=4] {'ep'}, dimensions={0} | all-to-all | bytes 4194304 | tf_op jit(solution)/shard_map/all_to_all | solution.py:174
  72.4 0.0 all-gather.5.cloned.1.call-update
  72.5 0.0 all-gather.7.cloned.1.call-start
  72.5 0.7 all-gather.7.cloned.1.call-update
  73.2 0.0 all-reduce.4.cloned.1.call-start
  73.3 56.7 %all-gather.5.cloned.1.call-done = bf16[8,256,2048]{2,1,0:T(8,128)(2,1)} async-done(((bf16[8,64,2048]{2,1,0:T(8,128)(2,1)}), bf16[8,256,2048]{2,1,0:T(8,128)(2,1)}) %all-gather.5.cloned.1.call-update) | async-done | bytes 8388624 | tf_op jit(solution)/shard_map/all_gather | solution.py:176
  129.9 5.9 %fusion.21 = f32[2048,256]{1,0:T(8,128)S(1)} fusion(bf16[2048,2048]{1,0:T(8,128)(2,1)} %bitcast.125, bf16[1,2048,256]{2,1,0:T(8,128)(2,1)S(1)} %copy-done.11), kind=kOutput, calls=%fused_computation.28 | convolution fusion | flops 2147483648 | bytes 11534336 | tf_op jit(solution)/shard_map/lrd,ldf->lrf/dot_general | solution.py:130
  135.8 0.1 copy-done.12
  135.9 2.6 fusion.4
  138.6 5.6 %convert_bitcast_fusion = bf16[1,8,4,64,2048]{4,3,2,1,0:T(8,128)(2,1)} fusion(bf16[8,4,64,256]{3,2,1,0:T(8,128)(2,1)S(1)} %bitcast.113, bf16[1,256,2048]{2,1,0:T(8,128)(2,1)S(1)} %copy-done), kind=kOutput, calls=%fused_computation.3 | convolution fusion | flops 2151677952 | bytes 10485760 | tf_op jit(solution)/shard_map/lrf,lfd->lrd/dot_general | solution.py:133
  144.1 0.0 copy-start.6
  144.1 0.0 copy-start.13
  144.2 0.0 all-reduce.4.cloned.1.call-update
  144.2 0.2 reduce-scatter.5.cloned.1.call-start
  144.4 0.6 copy-done.4
  145.0 0.1 copy.39
  145.2 0.1 fusion.29
  145.5 0.1 fusion.34
  145.6 0.1 dynamic-slice.2
  145.7 0.6 dynamic-slice
  146.3 8.4 %all-gather.7.cloned.1.call-done = bf16[512,2048]{1,0:T(8,128)(2,1)} async-done(((bf16[128,2048]{1,0:T(8,128)(2,1)}), bf16[512,2048]{1,0:T(8,128)(2,1)}) %all-gather.7.cloned.1.call-update) | async-done | bytes 2097168 | tf_op jit(solution)/shard_map/all_gather | solution.py:182
  154.6 3.5 fusion.56
  158.2 5.4 %convolution_convert_fusion = bf16[512,2048]{1,0:T(8,128)(2,1)} fusion(bf16[256,2048]{1,0:T(8,128)(2,1)} %param.29, bf16[512,2048]{1,0:T(8,128)(2,1)S(1)} %copy-done.10, bf16[2048,256]{1,0:T(8,128)(2,1)} %param.28, f32[512,256]{1,0:T(8,128)} %fusion.56), kind=kOutput, calls=%fused_computation.9 | convolution fusion | flops 1075576832 | bytes 6815744 | tf_op jit(solution)/shard_map/dot_general | solution.py:140
  163.5 0.0 reduce-scatter.5.cloned.1.call-update
  163.5 146.5 %all-reduce.4.cloned.1.call-done = bf16[1,8,4,64,2048]{4,3,2,1,0:T(8,128)(2,1)} async-done(((bf16[1,8,4,64,2048]{4,3,2,1,0:T(8,128)(2,1)}), bf16[1,8,4,64,2048]{4,3,2,1,0:T(8,128)(2,1)}) %all-reduce.4.cloned.1.call-update) | async-done | bytes 8388624
  310.0 2.5 constant_dynamic-slice_fusion
  312.5 5.2 %copy.56 = bf16[1,512,2048]{2,0,1:T(2,128)(2,1)} copy(bf16[1,512,2048]{2,1,0:T(8,128)(2,1)S(1)} %bitcast.111) | data formatting | bytes 4194304 | tf_op jit(solution)/shard_map/reshape | solution.py:207
  317.7 0.5 broadcast.377
  318.2 13.2 %reduce.9 = bf16[512,2048]{1,0:T(8,128)(2,1)S(1)} reduce(bf16[512,1,2048]{2,1,0:T(2,128)(2,1)} %bitcast.108, bf16[]{:T(256)} %broadcast.377), dimensions={1}, to_apply=%bitcast.106.reduce_sub_computation | reduce | bytes 4194306
  331.4 3.8 reshape.653
  335.2 5.6 %all-to-all-start.1 = ((bf16[8,2,65536]{2,1,0:T(2,128)(2,1)}), bf16[8,2,65536]{2,1,0:T(2,128)(2,1)S(1)}, u32[]{:S(2)}, u32[]{:S(2)}) async-start(bf16[8,2,65536]{2,1,0:T(2,128)(2,1)} %reshape.653), calls=%async_computation.1 | async-start | bytes 4194304 | tf_op jit(solution)/shard_map/all_to_all | solution.py:210
  340.9 0.1 copy.43
  341.0 0.1 fusion.45
  341.1 0.1 fusion.40
  341.3 0.1 copy.40
  341.4 0.1 fusion.41
  341.7 68.2 %all_gather.9 = bf16[2048,128]{0,1:T(8,128)(2,1)S(1)} all-gather(bf16[256,128]{0,1:T(8,128)(2,1)S(1)} %bitcast.119), channel_id=1, replica_groups=mesh['ep'=8,'tp'=4] {'ep'}, dimensions={0}, use_global_device_ids=true | all-gather | bytes 589824 | tf_op jit(solution)/shard_map/all_gather | solution.py:92
  409.9 1.4 multiply_reduce_fusion
  411.3 1.9 fusion
  413.2 1.7 fusion.12
  414.9 0.1 reshape.594
  415.0 0.8 copy.47
  415.8 0.0 all-to-all-done.1
  415.8 4.4 reshape.654
  420.2 3.5 copy.55
  423.7 2.3 gather_fusion.1
  426.0 2.5 reshape.614
  428.5 4.1 multiply_reduce_fusion.1
  432.5 2.3 fusion.18
  (54 shorter events, 0.6 us)
Async XLA Ops:
  7.2 131.4 %copy-start = (bf16[1,256,2048]{2,1,0:T(8,128)(2,1)S(1)}, bf16[1,256,2048]{2,1,0:T(8,128)(2,1)}, u32[]{:S(2)}) copy-start(bf16[1,256,2048]{2,1,0:T(8,128)(2,1)} %param.26) | copy-start | bytes 3145732
  7.2 122.7 %all-gather.5.cloned.1.call-start = ((), (), s32[]{:S(2)}) async-start(), calls=%async_computation.4 | async-start | bytes 10485760 | tf_op jit(solution)/shard_map/all_gather | solution.py:176
  13.4 3.4 copy-start.2
  72.4 57.5 %copy-start.11 = (bf16[1,2048,256]{2,1,0:T(8,128)(2,1)S(1)}, bf16[1,2048,256]{2,1,0:T(8,128)(2,1)}, u32[]{:S(2)}) copy-start(bf16[1,2048,256]{2,1,0:T(8,128)(2,1)} %param.24) | copy-start | bytes 3145732
  72.5 82.2 %all-gather.7.cloned.1.call-start = ((), (), s32[]{:S(2)}) async-start(), calls=%async_computation.5 | async-start | bytes 2621440 | tf_op jit(solution)/shard_map/all_gather | solution.py:182
  73.2 236.8 %all-reduce.4.cloned.1.call-start = ((), (), s32[]{:S(2)}) async-start(), calls=%async_computation.6 | async-start | bytes 16777216
  129.9 5.9 %copy-start.9 = (bf16[8,256,2048]{2,1,0:T(8,128)(2,1)S(1)}, bf16[8,256,2048]{2,1,0:T(8,128)(2,1)}, u32[]{:S(2)}) copy-start(bf16[8,256,2048]{2,1,0:T(8,128)(2,1)} %all-gather.5.cloned.1.call-done) | copy-start | bytes 25165828
  129.9 6.0 %copy-start.12 = (bf16[1,2048,256]{2,1,0:T(8,128)(2,1)S(1)}, bf16[1,2048,256]{2,1,0:T(8,128)(2,1)}, u32[]{:S(2)}) copy-start(bf16[1,2048,256]{2,1,0:T(8,128)(2,1)} %param.25) | copy-start | bytes 3145732
  144.1 0.9 copy-start.4
  144.1 1.1 copy-start.7
  144.1 1.3 copy-start.3
  144.1 1.3 copy-start.8
  144.1 1.4 copy-start.6
  144.1 1.5 copy-start.13
  144.2 288.4 %reduce-scatter.5.cloned.1.call-start = ((), (), s32[]{:S(2)}) async-start(), calls=%async_computation.3 | async-start | bytes 2621440 | tf_op jit(solution)/shard_map/reduce_scatter | solution.py:200
  154.6 3.5 copy-start.10
  335.2 6.4 %copy-start.5 = (bf16[256,64]{0,1:T(8,128)(2,1)S(1)}, bf16[256,64]{0,1:T(8,128)(2,1)}, u32[]{:S(2)}) copy-start(bf16[256,64]{0,1:T(8,128)(2,1)} %param.17) | copy-start | bytes 98308
  335.2 80.5 %all-to-all-start.1 = ((bf16[8,2,65536]{2,1,0:T(2,128)(2,1)}), bf16[8,2,65536]{2,1,0:T(2,128)(2,1)S(1)}, u32[]{:S(2)}, u32[]{:S(2)}) async-start(bf16[8,2,65536]{2,1,0:T(2,128)(2,1)} %reshape.653), calls=%async_computation.1 | async-start | bytes 4194304 | tf_op jit(solution)/shard_map/all_to_all | solution.py:210
  426.0 8.8 %copy-start.1 = (bf16[1,256,2048]{2,1,0:T(8,128)(2,1)S(1)}, bf16[1,256,2048]{2,1,0:T(8,128)(2,1)}, u32[]{:S(2)}) copy-start(bf16[1,256,2048]{2,1,0:T(8,128)(2,1)} %param.26) | copy-start | bytes 3145732
Sparse Core Ops, SparseCore 0:
  72.6 57.2 all-gather.4
  132.0 22.5 all-gather.6
  157.1 152.8 all-reduce.3
  312.4 31.3 reduce-scatter.4
where the time goes:
time: 442 us; the launch traced here: 441 us
  waiting for transfers between devices  212 us (48%)
  blocking collectives  124 us (28%)
  local copies, waits for them, and re-layouts  33 us (7%)
  other arithmetic  26.2 us (6%)
  matrix products  26 us (6%)
  between operations  14.2 us (3%)
  starting transfers between devices  5.97 us (1%)
    unnamed x5, waiting for transfers between devices  147 us
    all_gather x1, blocking collectives, attend(): piece_rows = lax.all_gather(key_value, 'ep', axis=0, tiled=True)  68.2 us
    all_gather x1, waiting for transfers between devices, experts_half(): lax.all_gather(landed.reshape(local_experts, ep_size, 1, capacity, model_...  56.7 us
    all_to_all x1, blocking collectives, experts_half(): landed = lax.all_to_all(send, 'ep', split_axis=0, concat_axis=1, tiled=True)  55.6 us
    unnamed x37, local copies, waits for them, and re-layouts  16.9 us
    unnamed x1, other arithmetic  13.2 us
  transfers between devices with their start and end apart: 5, of which 3 were waited for; matrix products, arithmetic and copies ran while one was open for 16% of the time, Pallas kernels for 0%

commit v1 on v0

v1 whole, which is shorter than its diff:
```python
import functools

import jax
import jax.numpy as jnp
from jax import lax
from jax.experimental import pallas as pl
from jax.experimental.pallas import tpu as pltpu
from jax.sharding import PartitionSpec as P

GRID_W = 64
MESH = pl.DeviceIdType.MESH


epsilon = 1e-06
rotary_base = 10000.0
routed_scale = 2.5


def exchange_kernel(plan, sizes, *refs):
    count = len(plan)
    sources, targets = refs[:count], refs[count : 2 * count]
    send_sems = refs[2 * count : 3 * count]
    recv_sems = refs[3 * count : 4 * count]
    own_sems = refs[4 * count]
    axes = []
    for axis, _ in plan:
        if axis not in axes:
            axes.append(axis)
    barrier = pltpu.get_barrier_semaphore()
    for axis in axes:
        me, n = lax.axis_index(axis), sizes[axis]

        def greet(i, c, axis=axis, me=me, n=n):
            pl.semaphore_signal(
                barrier, inc=1, device_id={axis: lax.rem(me + i, n)}, device_id_type=MESH
            )
            return c

        lax.fori_loop(1, n, greet, 0)
    pl.semaphore_wait(barrier, sum(sizes[axis] - 1 for axis in axes))

    def copy_of(k, i):
        axis, scattered = plan[k]
        me, n = lax.axis_index(axis), sizes[axis]
        peer = lax.rem(me + i, n)
        return pltpu.make_async_remote_copy(
            src_ref=sources[k].at[peer] if scattered else sources[k],
            dst_ref=targets[k].at[me],
            send_sem=send_sems[k].at[i],
            recv_sem=recv_sems[k].at[i],
            device_id={axis: peer},
            device_id_type=MESH,
        )

    for k, (axis, scattered) in enumerate(plan):

        def begin(i, c, k=k):
            copy_of(k, i).start()
            return c

        lax.fori_loop(1, sizes[axis], begin, 0)
    local = []
    for k, (axis, scattered) in enumerate(plan):
        me = lax.axis_index(axis)
        copy = pltpu.make_async_copy(
            sources[k].at[me] if scattered else sources[k], targets[k].at[me], own_sems.at[k]
        )
        copy.start()
        local.append(copy)
    for copy in local:
        copy.wait()
    for k, (axis, scattered) in enumerate(plan):

        def finish(i, c, k=k):
            copy_of(k, i).wait()
            return c

        lax.fori_loop(1, sizes[axis], finish, 0)


def exchange(operands, plan, number):
    sizes = {axis: lax.axis_size(axis) for axis, _ in plan}
    shapes = []
    for array, (axis, scattered) in zip(operands, plan):
        shape = array.shape if scattered else (sizes[axis],) + array.shape
        shapes.append(jax.ShapeDtypeStruct(shape, array.dtype))
    sems = [pltpu.SemaphoreType.DMA((sizes[axis],)) for axis, _ in plan]
    traffic = 2 * sum(s.size * s.dtype.itemsize for s in shapes)
    return pl.pallas_call(
        functools.partial(exchange_kernel, plan, sizes),
        out_shape=shapes,
        in_specs=[pl.BlockSpec(memory_space=pl.ANY)] * len(plan),
        out_specs=[pl.BlockSpec(memory_space=pl.ANY)] * len(plan),
        scratch_shapes=sems + sems + [pltpu.SemaphoreType.DMA((len(plan),))],
        compiler_params=pltpu.CompilerParams(collective_id=number, has_side_effects=True),
        cost_estimate=pl.CostEstimate(
            flops=0, bytes_accessed=16 * traffic, transcendentals=0
        ),
    )(*operands)


def rotate_heads(heads_in, gain_row, positions):
    values32 = heads_in.astype(jnp.float32)
    scaled = (
        values32
        * lax.rsqrt(jnp.mean(values32 * values32, axis=-1, keepdims=True) + epsilon)
        * gain_row
    )
    pair_count = scaled.shape[-1] // 4
    inv_freq = rotary_base ** (-jnp.arange(pair_count, dtype=jnp.float32) / pair_count)
    grid_row = (positions // GRID_W).astype(jnp.float32)
    grid_col = (positions % GRID_W).astype(jnp.float32)
    angles = jnp.concatenate([grid_row[:, None] * inv_freq, grid_col[:, None] * inv_freq], axis=-1)[
        :, None, :
    ]
    cosine = jnp.cos(angles)
    sine_part = jnp.sin(angles)
    first_half = scaled[..., 0::2]
    second_half = scaled[..., 1::2]
    turned = jnp.stack(
        [
            first_half * cosine - second_half * sine_part,
            first_half * sine_part + second_half * cosine,
        ],
        axis=-1,
    )
    return turned.reshape(scaled.shape).astype(jnp.bfloat16)


def span_length(row_count):
    length = min(row_count, 2048)
    while row_count % length:
        length -= 1
    return length


def rotated(query_rows, key_rows, value_rows, query_gain, key_gain):
    row_count = query_rows.shape[0]
    head_size = query_gain.shape[0]
    q_heads = query_rows.shape[1] // head_size
    kv_heads = key_rows.shape[1] // head_size
    positions = lax.axis_index("ep") * row_count + jnp.arange(row_count, dtype=jnp.int32)
    q_rot = rotate_heads(query_rows.reshape(row_count, q_heads, head_size), query_gain, positions)
    k_rot = rotate_heads(key_rows.reshape(row_count, kv_heads, head_size), key_gain, positions)
    key_value = jnp.stack([k_rot, value_rows.reshape(row_count, kv_heads, head_size)], axis=2)
    return q_rot, key_value.reshape(row_count, kv_heads * 2 * head_size)


def attend(q_rot, piece_rows):
    row_count, q_heads, head_size = q_rot.shape
    kv_heads = piece_rows.shape[1] // (2 * head_size)
    group = q_heads // kv_heads
    scale = head_size ** (-0.5)
    q_grouped = q_rot.reshape(row_count, kv_heads, group, head_size).transpose(1, 2, 0, 3)
    q_grouped = q_grouped.reshape(kv_heads, group * row_count, head_size)
    query_count = group * row_count
    initial = (
        jnp.full((kv_heads, query_count), -jnp.inf, jnp.float32),
        jnp.zeros((kv_heads, query_count), jnp.float32),
        jnp.zeros((kv_heads, query_count, head_size), jnp.float32),
    )

    def one_span(carried, span_rows):
        run_max, run_sum, mixed = carried
        keys_span = span_rows[:, :, 0, :]
        values_span = span_rows[:, :, 1, :]
        scores = (
            jnp.einsum("hrd,shd->hrs", q_grouped, keys_span, preferred_element_type=jnp.float32)
            * scale
        )
        new_max = jnp.maximum(run_max, jnp.max(scores, axis=-1))
        factor = jnp.exp(run_max - new_max)
        weights = jnp.exp(scores - new_max[..., None])
        run_sum = run_sum * factor + jnp.sum(weights, axis=-1)
        added = jnp.einsum(
            "hrs,shd->hrd",
            weights.astype(jnp.bfloat16),
            values_span,
            preferred_element_type=jnp.float32,
        )
        mixed = mixed * factor[..., None] + added
        return ((new_max, run_sum, mixed), None)

    piece_count = piece_rows.shape[0]
    length = span_length(piece_count)
    spans = piece_rows.reshape(piece_count // length, length, kv_heads, 2, head_size)
    carried, unused = lax.scan(one_span, initial, spans)
    run_max, run_sum, mixed = carried
    result = (mixed / run_sum[..., None]).astype(jnp.bfloat16)
    result = result.reshape(kv_heads, group, row_count, head_size).transpose(2, 0, 1, 3)
    return result.reshape(row_count, q_heads * head_size)


def slot_numbers(own_routes, experts, capacity):
    tok_rows = own_routes.shape[0]
    named = own_routes[:, :, None] == jnp.arange(experts, dtype=jnp.int32)
    counts = jnp.any(named, axis=1).astype(jnp.bfloat16)
    rows = jnp.arange(tok_rows, dtype=jnp.int32)
    before = (rows[:, None] > rows[None, :]).astype(jnp.bfloat16)
    earlier = jnp.dot(before, counts, preferred_element_type=jnp.float32)
    ranks = jnp.sum(jnp.where(named, earlier[:, None, :], 0.0), axis=2).astype(jnp.int32)
    return own_routes * capacity + ranks


def hidden_of(rows_in, w_gate, w_up):
    gate_proj = jnp.einsum("...rd,...df->...rf", rows_in, w_gate, preferred_element_type=jnp.float32)
    up_proj = jnp.einsum("...rd,...df->...rf", rows_in, w_up, preferred_element_type=jnp.float32)
    return (jax.nn.silu(gate_proj) * up_proj).astype(jnp.bfloat16)


def body(
    query_rows,
    key_rows,
    value_rows,
    query_gain,
    key_gain,
    moe_tokens,
    norm_gain,
    routes,
    route_weights,
    expert_gate,
    expert_up,
    expert_down,
    shared_gate,
    shared_up,
    shared_down,
):
    tok_rows, model_width = moe_tokens.shape
    top_count = routes.shape[1]
    tp_size = lax.axis_size("tp")
    ep_size = lax.axis_size("ep")
    local_experts = expert_gate.shape[0]
    experts = local_experts * ep_size
    capacity = 2 * tok_rows * top_count // experts
    lane = lax.axis_index("tp")

    all_gate = lax.all_gather(expert_gate, "tp", axis=0)
    all_up = lax.all_gather(expert_up, "tp", axis=0)
    all_down = lax.all_gather(expert_down, "tp", axis=0)

    values32 = moe_tokens.astype(jnp.float32)
    normed = (
        values32
        * lax.rsqrt(jnp.mean(values32 * values32, axis=-1, keepdims=True) + epsilon)
        * norm_gain
    ).astype(jnp.bfloat16)
    own_routes = lax.dynamic_slice_in_dim(routes, lane * tok_rows, tok_rows, 0)
    own_weights = lax.dynamic_slice_in_dim(route_weights, lane * tok_rows, tok_rows, 0)
    own_gates = own_weights / jnp.sum(own_weights, axis=-1, keepdims=True) * routed_scale
    slots = slot_numbers(own_routes, experts, capacity)
    slot_ids = jnp.arange(experts * capacity, dtype=jnp.int32)
    placing = jnp.any(slot_ids[:, None, None] == slots[None, :, :], axis=2).astype(jnp.bfloat16)
    send = jnp.dot(placing, normed, preferred_element_type=jnp.float32).astype(jnp.bfloat16)
    send = send.reshape(ep_size, local_experts * capacity, model_width)

    q_rot, key_value = rotated(query_rows, key_rows, value_rows, query_gain, key_gain)

    arrived, group_rows, pieces = exchange(
        (send, normed, key_value), (("ep", True), ("tp", False), ("ep", False)), 1
    )
    attn_out = attend(q_rot, pieces.reshape(-1, pieces.shape[-1]))
    shared_hidden = hidden_of(
        group_rows.reshape(tp_size * tok_rows, model_width), shared_gate, shared_up
    )
    shared_part = jnp.dot(shared_hidden, shared_down, preferred_element_type=jnp.float32)
    shared_part = shared_part.astype(jnp.bfloat16).reshape(tp_size, tok_rows, model_width)

    arrived = arrived.reshape(ep_size, local_experts, capacity, model_width).transpose(1, 0, 2, 3)
    arrived = arrived.reshape(local_experts, ep_size * capacity, model_width)
    total = 0.0
    for part in range(tp_size):
        hidden = hidden_of(arrived, all_gate[part], all_up[part])
        partial = jnp.einsum(
            "lrf,lfd->lrd", hidden, all_down[part], preferred_element_type=jnp.float32
        )
        total = total + partial.astype(jnp.bfloat16).astype(jnp.float32)
    outgoing = total.astype(jnp.bfloat16).reshape(local_experts, ep_size, capacity, model_width)
    outgoing = outgoing.transpose(1, 0, 2, 3).reshape(
        ep_size, local_experts * capacity, model_width
    )
    returned, shared_parts = exchange((outgoing, shared_part), (("ep", True), ("tp", True)), 2)

    flat_rows = returned.reshape(experts * capacity, model_width)
    moe_out = jnp.sum(shared_parts.astype(jnp.float32), axis=0)
    for k in range(top_count):
        choosing = (slots[:, k, None] == slot_ids[None, :]).astype(jnp.bfloat16)
        picked = jnp.dot(choosing, flat_rows, preferred_element_type=jnp.float32)
        moe_out = moe_out + own_gates[:, k, None] * picked
    return (attn_out, moe_out.astype(jnp.bfloat16))


def solution(mesh):
    return jax.shard_map(
        body,
        mesh=mesh,
        in_specs=(
            P("ep", "tp"),
            P("ep", "tp"),
            P("ep", "tp"),
            P(),
            P(),
            P(("ep", "tp"), None),
            P(),
            P("ep", None),
            P("ep", None),
            P("ep", None, "tp"),
            P("ep", None, "tp"),
            P("ep", "tp", None),
            P(None, "tp"),
            P(None, "tp"),
            P("tp", None),
        ),
        out_specs=(P("ep", "tp"), P(("ep", "tp"), None)),
        check_vma=False,
    )
```

time: 442 us -> 226 us (0.51)
  the two profiles are of different devices: /device:TPU:0 before, /device:TPU:11 now
where the time goes in v1:
time: 226 us
  Pallas kernels  111 us (49%)
  matrix products  46.8 us (21%)
  waiting for transfers between devices  41 us (18%)
  between operations  14.2 us (6%)
  other arithmetic  7.73 us (3%)
  local copies, waits for them, and re-layouts  5.11 us (2%)
    pallas_call x2, Pallas kernels, exchange(): pl.pallas_call(functools.partial(exchange_kernel, plan, sizes), out_shape...  111 us
    all_gather x1, waiting for transfers between devices, body(): all_down = lax.all_gather(expert_down, 'tp', axis=0)  36.1 us
    dot_general x4, matrix products, body(): jnp.einsum('lrf,lfd->lrd', hidden, all_down[part], preferred_element_type...  25.4 us
    dot_general x5, matrix products, hidden_of(): jnp.einsum('...rd,...df->...rf', rows_in, w_gate, preferred_element_type=...  8.9 us
    dot_general x1, matrix products, body(): jnp.dot(shared_hidden, shared_down, preferred_element_type=jnp.float32)  5.5 us
  transfers between devices with their start and end apart: 3, of which 2 were waited for; matrix products, arithmetic and copies ran while one was open for 13% of the time, Pallas kernels for 27%

profile of v1, /device:TPU:11, one launch (start us, length us, event | category | flops | bytes accessed | tf_op | source)
XLA Modules:
  0.0 226.1 jit_solution(17982491104220814858)
XLA Ops:
  7.2 0.0 copy-start
  7.2 0.0 copy-start.6
  7.2 0.0 copy-start.4
  7.2 0.0 copy-start.7
  7.2 0.0 copy-start.3
  7.2 0.0 copy-start.5
  7.2 0.0 all-gather.7.cloned.1.call-start
  7.3 0.7 all-gather.7.cloned.1.call-update
  8.0 0.0 all-gather.9.cloned.1.call-start
  8.0 0.7 all-gather.9.cloned.1.call-update
  8.7 0.0 all-gather.11.cloned.1.call-start
  8.8 0.7 all-gather.11.cloned.1.call-update
  9.5 0.8 fusion.64
  10.3 0.8 fusion.66
  11.1 1.0 copy.45
  12.2 0.7 fusion.55
  13.1 0.1 fusion.77
  13.2 0.1 fusion.74
  13.4 0.0 copy-done.6
  13.4 0.0 copy-done.4
  13.4 0.1 fusion.73
  13.7 0.0 copy-done.7
  13.7 0.7 copy.48.refs_2_
  14.4 0.1 copy.46
  14.6 0.1 fusion.69
  14.7 0.1 fusion.53
  14.8 0.0 copy-done.3
  14.8 0.2 fusion.21
  15.0 0.0 copy-done.5
  15.0 0.2 fusion.23.refs_1_
  15.2 0.0 copy-start.2
  15.2 2.0 convolution_convert_fusion.5
  17.3 0.0 copy-done.2
  17.3 61.1 %shard_map.158 = (bf16[8,64,2048]{2,1,0:T(8,128)(2,1)}, bf16[4,128,2048]{2,1,0:T(8,128)(2,1)}, bf16[8,256,128]{2,1,0:T(8,128)(2,1)}) custom-call(bf16[8,64,2048]{2,1,0:T(8,128)(2,1)} %bitcast.121, bf16[128,2048]{1,0:T(8,128)(2,1)} %copy-done.2, bf16[256,128]{1,0:T(8,128)(2,1)} %copy.48.refs_2_), custom_call_target="tpu_custom_call" | custom-call | bytes 150994944 | tf_op jit(solution)/shard_map/pallas_call | solution.py:89
  78.3 1.5 copy.49
  79.8 0.2 squeeze.9
  80.1 1.4 multiply_reduce_fusion
  81.4 2.1 fusion
  83.6 0.0 copy-start.10
  83.6 1.7 fusion.18
  85.3 0.1 reshape.469
  85.4 0.8 copy.51
  86.2 0.0 copy-done.10
  86.2 2.3 %fusion.89 = f32[512,256]{1,0:T(8,128)S(1)} fusion(bf16[512,2048]{1,0:T(8,128)(2,1)} %bitcast.137, bf16[2048,256]{1,0:T(8,128)(2,1)S(1)} %copy-done.10), kind=kOutput, calls=%fused_computation.156 | convolution fusion | flops 536870912 | bytes 3670016 | tf_op jit(solution)/shard_map/...rd,...df->...rf/dot_general | solution.py:206
  88.5 0.0 copy-done
  88.5 5.5 %convolution_convert_fusion = bf16[512,2048]{1,0:T(8,128)(2,1)} fusion(bf16[256,2048]{1,0:T(8,128)(2,1)S(1)} %copy-done, bf16[512,2048]{1,0:T(8,128)(2,1)} %bitcast.138, bf16[2048,256]{1,0:T(8,128)(2,1)} %param.28, f32[512,256]{1,0:T(8,128)S(1)} %fusion.89), kind=kOutput, calls=%fused_computation.7 | convolution fusion | flops 1075576832 | bytes 6815744 | tf_op jit(solution)/shard_map/dot_general | solution.py:265
  94.0 2.7 %fusion.24 = f32[512,256]{1,0:T(8,128)S(1)} fusion(bf16[512,2048]{1,0:T(8,128)(2,1)} %bitcast.129, bf16[4,2048,256]{2,1,0:T(8,128)(2,1)} %all-gather.7.cloned.1.call-done), kind=kOutput, calls=%fused_computation.39 | convolution fusion | flops 536870912 | bytes 3670016 | tf_op jit(solution)/shard_map/...rd,...df->...rf/dot_general | solution.py:206
  96.7 0.4 copy-done.8
  97.1 2.4 %fusion.25 = f32[512,256]{1,0:T(8,128)S(1)} fusion(bf16[512,2048]{1,0:T(8,128)(2,1)} %bitcast.130, bf16[4,2048,256]{2,1,0:T(8,128)(2,1)S(1)} %copy-done.8), kind=kOutput, calls=%fused_computation.43 | convolution fusion | flops 536870912 | bytes 3670016 | tf_op jit(solution)/shard_map/...rd,...df->...rf/dot_general | solution.py:206
  99.6 0.0 copy-done.9
  99.6 0.7 fusion.26
  100.3 0.7 fusion.27
  101.0 2.9 %all-gather.9.cloned.1.call-done = bf16[4,2048,256]{2,1,0:T(8,128)(2,1)} async-done(((bf16[1,2048,256]{2,1,0:T(8,128)(2,1)}), bf16[4,2048,256]{2,1,0:T(8,128)(2,1)}) %all-gather.9.cloned.1.call-update) | async-done | bytes 4194320 | tf_op jit(solution)/shard_map/all_gather | solution.py:238
  103.9 36.1 %all-gather.11.cloned.1.call-done = bf16[4,256,2048]{2,1,0:T(8,128)(2,1)} async-done(((bf16[1,256,2048]{2,1,0:T(8,128)(2,1)}), bf16[4,256,2048]{2,1,0:T(8,128)(2,1)}) %all-gather.11.cloned.1.call-update) | async-done | bytes 4194320 | tf_op jit(solution)/shard_map/all_gather | solution.py:239
  140.0 5.8 %convolution_convert_fusion.3 = bf16[512,2048]{1,0:T(8,128)(2,1)} fusion(bf16[512,2048]{1,0:T(8,128)(2,1)} %bitcast.131, bf16[4,256,2048]{2,1,0:T(8,128)(2,1)} %all-gather.11.cloned.1.call-done, bf16[4,2048,256]{2,1,0:T(8,128)(2,1)} %all-gather.9.cloned.1.call-done, f32[512,256]{1,0:T(8,128)S(1)} %fusion.26), kind=kOutput, calls=%fused_computation.10 | convolution fusion | flops 1075576832 | bytes 6815744 | tf_op jit(solution)/shard_map/lrf,lfd->lrd/dot_general | solution.py:273
  145.8 5.9 %convolution_convert_fusion.2 = bf16[512,2048]{1,0:T(8,128)(2,1)} fusion(bf16[512,2048]{1,0:T(8,128)(2,1)} %bitcast.132, bf16[4,256,2048]{2,1,0:T(8,128)(2,1)} %all-gather.11.cloned.1.call-done, bf16[4,2048,256]{2,1,0:T(8,128)(2,1)} %all-gather.9.cloned.1.call-done, f32[512,256]{1,0:T(8,128)S(1)} %fusion.25), kind=kOutput, calls=%fused_computation.9 | convolution fusion | flops 1075576832 | bytes 6815744 | tf_op jit(solution)/shard_map/lrf,lfd->lrd/dot_general | solution.py:273
  151.6 5.8 %convolution_convert_fusion.1 = bf16[512,2048]{1,0:T(8,128)(2,1)} fusion(bf16[512,2048]{1,0:T(8,128)(2,1)} %bitcast.133, bf16[4,256,2048]{2,1,0:T(8,128)(2,1)} %all-gather.11.cloned.1.call-done, bf16[4,2048,256]{2,1,0:T(8,128)(2,1)} %all-gather.9.cloned.1.call-done, f32[512,256]{1,0:T(8,128)S(1)} %fusion.24), kind=kOutput, calls=%fused_computation.8 | convolution fusion | flops 1075576832 | bytes 6815744 | tf_op jit(solution)/shard_map/lrf,lfd->lrd/dot_general | solution.py:273
  157.5 7.9 %add_convert_fusion = bf16[512,2048]{1,0:T(8,128)(2,1)} fusion(bf16[512,2048]{1,0:T(8,128)(2,1)} %convolution_convert_fusion.1, bf16[512,2048]{1,0:T(8,128)(2,1)} %convolution_convert_fusion.2, bf16[512,2048]{1,0:T(8,128)(2,1)} %convolution_convert_fusion.3, bf16[4,256,2048]{2,1,0:T(8,128)(2,1)} %all-gather.11.cloned.1.call-done, ...), kind=kOutput, calls=%fused_computation.5 | convolution fusion | flops 1083965440 | bytes 13107200 | tf_op jit(solution)/shard_map/lrf,lfd->lrd/dot_general | solution.py:273
  165.4 50.0 %shard_map.159 = (bf16[8,64,2048]{2,1,0:T(8,128)(2,1)}, bf16[4,128,2048]{2,1,0:T(8,128)(2,1)}) custom-call(bf16[8,64,2048]{2,1,0:T(8,128)(2,1)} %bitcast.123, bf16[4,128,2048]{2,1,0:T(8,128)(2,1)} %bitcast.122), custom_call_target="tpu_custom_call" | custom-call | bytes 134217728 | tf_op jit(solution)/shard_map/pallas_call | solution.py:89
  215.4 0.0 copy-start.1
  215.4 2.2 convert_reduce_fusion
  217.7 0.0 copy-done.1
  217.7 0.5 fusion.5
  218.2 1.3 fusion.6
  (30 shorter events, 0.5 us)
Async XLA Ops:
  7.2 81.3 %copy-start = (bf16[256,2048]{1,0:T(8,128)(2,1)S(1)}, bf16[256,2048]{1,0:T(8,128)(2,1)}, u32[]{:S(2)}) copy-start(bf16[256,2048]{1,0:T(8,128)(2,1)} %param.29) | copy-start | bytes 3145732
  7.2 6.2 %copy-start.6 = (s32[512,2]{0,1:T(2,128)S(1)}, s32[512,2]{0,1:T(2,128)}, u32[]{:S(2)}) copy-start(s32[512,2]{0,1:T(2,128)} %param.22) | copy-start | bytes 12292
  7.2 6.2 %copy-start.4 = (bf16[256,64]{0,1:T(8,128)(2,1)S(1)}, bf16[256,64]{0,1:T(8,128)(2,1)}, u32[]{:S(2)}) copy-start(bf16[256,64]{0,1:T(8,128)(2,1)} %param.17) | copy-start | bytes 98308
  7.2 6.5 %copy-start.7 = (f32[512,2]{0,1:T(2,128)S(1)}, f32[512,2]{0,1:T(2,128)}, u32[]{:S(2)}) copy-start(f32[512,2]{0,1:T(2,128)} %param.23) | copy-start | bytes 12292
  7.2 7.6 %copy-start.3 = (bf16[128,2048]{1,0:T(8,128)(2,1)S(1)}, bf16[128,2048]{1,0:T(8,128)(2,1)}, u32[]{:S(2)}) copy-start(bf16[128,2048]{1,0:T(8,128)(2,1)} %param.20) | copy-start | bytes 1572868
  7.2 7.8 %copy-start.5 = (f32[2048]{0:T(1024)S(1)}, f32[2048]{0:T(1024)}, u32[]{:S(2)}) copy-start(f32[2048]{0:T(1024)} %param.21) | copy-start | bytes 24580
  7.2 86.8 %all-gather.7.cloned.1.call-start = ((), (), s32[]{:S(2)}) async-start(), calls=%async_computation | async-start | bytes 5242880 | tf_op jit(solution)/shard_map/all_gather | solution.py:237
  8.0 96.0 %all-gather.9.cloned.1.call-start = ((), (), s32[]{:S(2)}) async-start(), calls=%async_computation.1 | async-start | bytes 5242880 | tf_op jit(solution)/shard_map/all_gather | solution.py:238
  8.7 131.3 %all-gather.11.cloned.1.call-start = ((), (), s32[]{:S(2)}) async-start(), calls=%async_computation.2 | async-start | bytes 5242880 | tf_op jit(solution)/shard_map/all_gather | solution.py:239
  15.2 2.0 copy-start.2
  83.6 2.6 %copy-start.10 = (bf16[2048,256]{1,0:T(8,128)(2,1)S(1)}, bf16[2048,256]{1,0:T(8,128)(2,1)}, u32[]{:S(2)}) copy-start(bf16[2048,256]{1,0:T(8,128)(2,1)} %param.27) | copy-start | bytes 3145732
  94.0 3.1 %copy-start.8 = (bf16[4,2048,256]{2,1,0:T(8,128)(2,1)S(1)}, bf16[4,2048,256]{2,1,0:T(8,128)(2,1)}, u32[]{:S(2)}) copy-start(bf16[4,2048,256]{2,1,0:T(8,128)(2,1)} %all-gather.7.cloned.1.call-done) | copy-start | bytes 12582916
  97.1 2.5 %copy-start.9 = (bf16[8,64,2048]{2,1,0:T(8,128)(2,1)S(1)}, bf16[8,64,2048]{2,1,0:T(8,128)(2,1)}, u32[]{:S(2)}) copy-start(bf16[8,64,2048]{2,1,0:T(8,128)(2,1)} %get-tuple-element.26) | copy-start | bytes 6291460
  215.4 2.3 copy-start.1
Sparse Core Ops, SparseCore 0:
  9.6 57.6 all-gather.6
  68.9 35.0 all-gather.8
  105.5 34.4 all-gather.10
